TPU v7x, 512 devices: a whole 4x8x8 slice. The times are simulated.
512 devices in a mesh: sp: 32 (over z, x), tp: 16 (over y, core).
Axes of the slice: x: 4, y: 8, z: 8, core: 2. Of those that a mesh axis runs over, the one named last changes fastest.
Arguments:
- lane_source_signal: bfloat16 [1024, 4096], P('tp', 'sp'), may hold values from -6 to 6
- spectral_damping_part: float32 [64, 64], P('tp'), may hold values from -3 to -0.0002
- spectral_angular_part: float32 [64, 64], P('tp'), may hold values from 0.31 to 201.0624
- interval_exponent: float32 [64], P('tp'), may hold values from -3.9 to -1.6
- entry_matrix_inphase: float32 [64, 64, 16], P('tp'), may hold values from -1 to 1
- entry_matrix_quadrature: float32 [64, 64, 16], P('tp'), may hold values from -1 to 1
- emission_inphase: float32 [64, 16, 64], P('tp'), may hold values from -0.75 to 0.75
- emission_quadrature: float32 [64, 16, 64], P('tp'), may hold values from -0.75 to 0.75
- lane_bypass_factor: float32 [1024], P('tp'), may hold values from -5 to 5
- spike_shrink_offset: float32 [64, 4096], P('tp', 'sp'), may hold values from -1.4 to 0
- lane_exit_matrix: bfloat16 [1024, 4096], P('tp'), may hold values from -0.1875 to 0.1875
- skipline_stream: bfloat16 [4096, 4096], P('sp'), may hold values from -6 to 6
- specialist_scaling_vector: float32 [4096], replicated, may hold values from 0.1 to 1.9
- selected_specialists: int32 [4096, 2], P('sp'), may hold values from 0 to 31, all different within a row; in each aligned block of 128 rows (0 to 127, 128 to 255, ...) at most 16 rows name the same one
- dispatcher_scores: float32 [4096, 2], P('sp'), may hold values from 0.1 to 1
- specialist_valve_matrix: bfloat16 [32, 4096, 2048], P('sp', None, 'tp'), may hold values from -0.09375 to 0.09375
- specialist_widen_matrix: bfloat16 [32, 4096, 2048], P('sp', None, 'tp'), may hold values from -0.09375 to 0.09375
- specialist_shrink_matrix: bfloat16 [32, 2048, 4096], P('sp', 'tp'), may hold values from -0.1875 to 0.1875
Outputs:
- updated: bfloat16 [4096, 4096], P('sp', 'tp')
Inputs may be any that keep to these rules, and one draw needn't show every extreme that they name: `selected_specialists`: each row names 2 different experts. Among the rows of each aligned block of 128 positions no expert is named more than 16 times, and in every block some expert is named exactly 16 times.
All inputs are finite; a program needn't handle non-finite values.
Results may differ from a plain program's by a relative error of at most 0.019.
Values may be sent and summed in bfloat16 or wider, within the bound.
A program may use at most 64 MiB of HBM per device.

v0:
```python
import jax
import jax.numpy as jnp
from jax import lax
from jax.sharding import PartitionSpec as P

EPS = 1e-06
PRECISE_MODE = lax.Precision.HIGHEST


def copy_for_each(array, axis):
    copies = jnp.broadcast_to(array, (lax.axis_size(axis), *array.shape))
    return lax.all_to_all(copies, axis, split_axis=0, concat_axis=0, tiled=True)


def gathered_once(array, axis):
    leaves = jax.tree.leaves(array)
    order = sorted(range(len(leaves)), key=lambda k: -leaves[k].size)
    width = (1, *leaves[order[0]].shape)[-1]
    lines = [
        jnp.pad(leaves[k].reshape(-1), (0, -leaves[k].size % width)).reshape(-1, width)
        for k in order
    ]
    both, at, found = (copy_for_each(jnp.concatenate(lines), axis), 0, {})
    for k, line in zip(order, lines):
        share = both[:, at : at + len(line)].reshape(len(both), -1)
        found[k] = share[:, : leaves[k].size].reshape(-1, *leaves[k].shape)
        at += len(line)
    numbers = iter(range(len(leaves)))
    return jax.tree.map(lambda _: found[next(numbers)], array)


def combined_pairwise(pieces, combine):
    while len(jax.tree.leaves(pieces)[0]) > 1:
        pieces = jax.vmap(combine)(
            *(jax.tree.map(lambda part: part[side::2], pieces) for side in (0, 1))
        )
    return jax.tree.map(lambda part: part[0], pieces)


def prefix(array, axis, combine, identity):
    length, mine = (lax.axis_size(axis), lax.axis_index(axis))
    passed = jnp.arange(length) < mine

    def kept(part, zero, own):
        part = jnp.where(
            passed.reshape(-1, *(1 for _ in own.shape)), part, jnp.asarray(zero, own.dtype)
        )
        return part

    pieces = gathered_once(array, axis)
    return combined_pairwise(jax.tree.map(kept, pieces, identity, array), combine)


def in_blocks(array, dim, length):
    before, after = (array.shape[:dim], array.shape[dim + 1 :])
    return jnp.moveaxis(array.reshape(*before, length, -1, *after), dim, 0)


def sent_and_summed(array, axis, dim):
    length = lax.axis_size(axis)
    parts = lax.all_to_all(in_blocks(array, dim, length), axis, 0, 0, tiled=True)
    return jnp.sum(parts.astype(jnp.float32), axis=0)


def taken_together(array, axis):
    return copy_for_each(array, axis).sum(axis=0)


def affine_pair(earlier, latter):
    mul_re = earlier[0] * latter[0] - earlier[1] * latter[1]
    mul_im = earlier[0] * latter[1] + earlier[1] * latter[0]
    add_re = latter[0] * earlier[2] - latter[1] * earlier[3] + latter[2]
    add_im = latter[0] * earlier[3] + latter[1] * earlier[2] + latter[3]
    return (mul_re, mul_im, add_re, add_im)


def local_prefix(elements):
    length = elements[0].shape[2]
    fills = (1.0, 0.0, 0.0, 0.0)
    offset = 1
    while offset < length:
        earlier = tuple(
            (
                jnp.pad(
                    item[:, :, : length - offset],
                    ((0, 0), (0, 0), (offset, 0)),
                    constant_values=fill,
                )
                for item, fill in zip(elements, fills)
            )
        )
        elements = affine_pair(earlier, elements)
        offset = offset * 2
    return elements


def per_device(
    lane_source_signal,
    spectral_damping_part,
    spectral_angular_part,
    interval_exponent,
    entry_matrix_inphase,
    entry_matrix_quadrature,
    emission_inphase,
    emission_quadrature,
    lane_bypass_factor,
    spike_shrink_offset,
    lane_exit_matrix,
    skipline_stream,
    specialist_scaling_vector,
    selected_specialists,
    dispatcher_scores,
    specialist_valve_matrix,
    specialist_widen_matrix,
    specialist_shrink_matrix,
):
    f32 = jnp.float32
    bf16 = jnp.bfloat16
    groups_here = spectral_damping_part.shape[0]
    lanes_within_bundle = entry_matrix_inphase.shape[2]
    tok_local = lane_source_signal.shape[1]
    bundled_signal = lane_source_signal.astype(f32).reshape(
        groups_here, lanes_within_bundle, tok_local
    )
    step_size = jnp.exp(interval_exponent)[:, None]
    natural_pace_exponent = spectral_damping_part * step_size
    angle = spectral_angular_part * step_size
    num_re = jnp.expm1(natural_pace_exponent) * jnp.cos(angle) - 2.0 * jnp.sin(0.5 * angle) ** 2
    num_im = jnp.exp(natural_pace_exponent) * jnp.sin(angle)
    denom = (
        spectral_damping_part * spectral_damping_part
        + spectral_angular_part * spectral_angular_part
    )
    fac_re = (num_re * spectral_damping_part + num_im * spectral_angular_part) / denom
    fac_im = (num_im * spectral_damping_part - num_re * spectral_angular_part) / denom
    map_re = (
        fac_re[:, :, None] * entry_matrix_inphase - fac_im[:, :, None] * entry_matrix_quadrature
    )
    map_im = (
        fac_re[:, :, None] * entry_matrix_quadrature + fac_im[:, :, None] * entry_matrix_inphase
    )
    drive_re = jnp.einsum("gpc,gct->gpt", map_re, bundled_signal, precision=PRECISE_MODE)
    drive_im = jnp.einsum("gpc,gct->gpt", map_im, bundled_signal, precision=PRECISE_MODE)
    recurrence_modulus = jnp.exp(
        natural_pace_exponent[:, :, None] + spike_shrink_offset[:, None, :]
    )
    trans_re = recurrence_modulus * jnp.cos(angle)[:, :, None]
    trans_im = recurrence_modulus * jnp.sin(angle)[:, :, None]
    cum_re, cum_im, state_real, state_imaginary = local_prefix(
        (trans_re, trans_im, drive_re, drive_im)
    )
    summary = (cum_re[:, :, -1], cum_im[:, :, -1], state_real[:, :, -1], state_imaginary[:, :, -1])
    unit = jnp.ones_like(summary[0])
    blank = jnp.zeros_like(summary[0])
    carried = prefix(summary, "sp", affine_pair, (unit, blank, blank, blank))
    enter_re = carried[2][:, :, None]
    enter_im = carried[3][:, :, None]
    state_real = state_real + cum_re * enter_re - cum_im * enter_im
    state_imaginary = state_imaginary + cum_re * enter_im + cum_im * enter_re
    value = (
        jnp.einsum("nef,nfi->nei", emission_inphase, state_real, precision=PRECISE_MODE)
        - jnp.einsum("nef,nfi->nei", emission_quadrature, state_imaginary, precision=PRECISE_MODE)
        + lane_bypass_factor.reshape(groups_here, lanes_within_bundle)[:, :, None] * bundled_signal
    )
    recurrence_result = (
        jax.nn.gelu(value).astype(bf16).reshape(groups_here * lanes_within_bundle, tok_local)
    )
    width = specialist_scaling_vector.shape[0]
    d_local = width // lax.axis_size("tp")
    col_start = lax.axis_index("tp") * d_local
    partial_rows = jnp.einsum(
        "ct,cd->td", recurrence_result, lane_exit_matrix, preferred_element_type=f32
    )
    projected_own = sent_and_summed(partial_rows.astype(jnp.bfloat16), "tp", 1).astype(bf16)
    own_residual = lax.dynamic_slice_in_dim(skipline_stream, col_start, d_local, 1)
    stream_own = (
        own_residual.astype(f32) + lax.optimization_barrier(projected_own).astype(f32)
    ).astype(bf16)
    own_stream = lax.optimization_barrier(stream_own).astype(f32)
    square_total = taken_together(jnp.sum(own_stream * own_stream, axis=1), "tp")
    inv_rms = lax.rsqrt(square_total / width + EPS)[:, None]
    own_gain = lax.dynamic_slice_in_dim(specialist_scaling_vector, col_start, d_local, 0)
    own_cols = (own_stream * inv_rms * own_gain).astype(bf16)
    share = dispatcher_scores / jnp.sum(dispatcher_scores, axis=1, keepdims=True)
    experts = lax.axis_size("sp")
    top = selected_specialists.shape[1]
    capacity = 2 * tok_local * top // experts
    flat_routes = selected_specialists.reshape(-1)
    hits = (flat_routes[:, None] == jnp.arange(experts, dtype=jnp.int32)[None, :]).astype(jnp.int32)
    ranks = jnp.sum((jnp.cumsum(hits, axis=0) - hits) * hits, axis=1)
    slot_ids = flat_routes * capacity + ranks
    slot_grid = jnp.arange(experts * capacity, dtype=jnp.int32)
    matched = slot_grid[:, None] == slot_ids[None, :]
    token_of = jnp.arange(tok_local * top, dtype=jnp.int32) // top
    slot_token = jnp.sum(jnp.where(matched, token_of[None, :], 0), axis=1)
    slot_live = jnp.any(matched, axis=1)
    gate_w = specialist_valve_matrix[0]
    up_w = specialist_widen_matrix[0]
    down_w = specialist_shrink_matrix[0]
    bf_zero = jnp.zeros((), bf16)
    dispatch = jnp.where(slot_live[:, None], own_cols[slot_token], bf_zero).reshape(
        experts, capacity, d_local
    )
    arrived = lax.all_to_all(dispatch, "sp", split_axis=0, concat_axis=0, tiled=True)
    piece = lax.all_gather(arrived, "tp", axis=2, tiled=True)
    gate_part = jnp.einsum("snd,df->snf", piece, gate_w, preferred_element_type=f32)
    up_part = jnp.einsum("snd,df->snf", piece, up_w, preferred_element_type=f32)
    hidden = (jax.nn.silu(gate_part) * up_part).astype(bf16)
    flat_hidden = hidden.reshape(experts * capacity, hidden.shape[2])
    down_part = jnp.dot(flat_hidden, down_w, preferred_element_type=f32).astype(bf16)
    summed = lax.psum_scatter(
        down_part.astype(f32).astype(jnp.bfloat16), "tp", scatter_dimension=1, tiled=True
    ).astype(jnp.float32)
    expert_out = summed.astype(bf16).reshape(experts, capacity, d_local)
    returned = lax.all_to_all(expert_out, "sp", split_axis=0, concat_axis=0, tiled=True).reshape(
        experts * capacity, d_local
    )
    picked = returned[slot_ids].reshape(tok_local, top, d_local)
    combined = jnp.sum(lax.optimization_barrier(picked).astype(f32) * share[:, :, None], axis=1)
    return (own_stream + combined).astype(bf16)


def solution(mesh):
    placed = (
        P("tp", "sp"),
        P("tp", None),
        P("tp", None),
        P("tp"),
        P("tp", None, None),
        P("tp", None, None),
        P("tp", None, None),
        P("tp", None, None),
        P("tp"),
        P("tp", "sp"),
        P("tp", None),
        P("sp", None),
        P(),
        P("sp", None),
        P("sp", None),
        P("sp", None, "tp"),
        P("sp", None, "tp"),
        P("sp", "tp", None),
    )
    return jax.shard_map(
        per_device, mesh=mesh, in_specs=placed, out_specs=P("sp", "tp"), check_vma=False
    )
```

profile of v0, /device:TPU:25, one launch (start us, length us, event | category | flops | bytes accessed | tf_op | source)
XLA Modules:
  0.0 256.6 jit_solution(5773878891755166815)
XLA Ops:
  6.5 0.7 exp.13
  7.3 0.8 fusion.57
  8.1 1.1 fusion.42
  9.2 1.1 fusion.46
  10.3 0.9 subtract_add_fusion.6
  11.2 1.0 add_add_fusion.5
  12.3 0.2 add_add_fusion.4
  12.7 0.2 add_add_fusion.3
  13.1 0.2 add_add_fusion.2
  13.4 0.2 add_add_fusion.1
  13.8 0.2 add_add_fusion
  14.0 0.2 multiply_subtract_fusion
  14.2 0.3 slice_reduce_fusion.1
  14.5 0.3 slice_reduce_fusion
  14.8 0.8 reshape.198
  15.6 12.9 %all-to-all-start = ((f32[32,1,1024]{2,1,0:T(1,128)}), f32[32,1,1024]{2,1,0:T(1,128)S(1)}, u32[]{:S(2)}, u32[]{:S(2)}) async-start(f32[32,1,1024]{2,1,0:T(1,128)} %reshape.198), calls=%async_computation | async-start | bytes 262144 | tf_op jit(solution)/shard_map/all_to_all | solution.py:12
  28.6 9.2 %all-to-all-done = f32[32,1,1024]{2,1,0:T(1,128)S(1)} async-done(((f32[32,1,1024]{2,1,0:T(1,128)}), f32[32,1,1024]{2,1,0:T(1,128)S(1)}, u32[]{:S(2)}, u32[]{:S(2)}) %all-to-all-start) | async-done | bytes 131104 | tf_op jit(solution)/shard_map/all_to_all | solution.py:12
  37.9 0.5 broadcast.191
  38.4 0.9 reduce.12
  39.7 0.3 fusion.16
  40.1 0.4 fusion.36
  40.5 0.4 convolution_convert_fusion.1
  40.9 1.1 copy.117
  42.0 9.1 %all-to-all-start.1 = ((bf16[16,128,256]{2,1,0:T(8,128)(2,1)}), bf16[16,128,256]{2,1,0:T(8,128)(2,1)S(1)}, u32[]{:S(2)}, u32[]{:S(2)}) async-start(bf16[16,128,256]{2,1,0:T(8,128)(2,1)} %bitcast.68), calls=%async_computation.1 | async-start | bytes 2097152 | tf_op jit(solution)/shard_map/all_to_all | solution.py:61
  51.4 0.1 reshape.168
  51.6 0.6 reduce-window.6
  52.2 0.2 slice_reduce_fusion.4
  52.5 0.2 fusion.7
  52.7 0.2 select_reduce_fusion
  52.9 24.5 %all-to-all-done.1 = bf16[16,128,256]{2,1,0:T(8,128)(2,1)S(1)} async-done(((bf16[16,128,256]{2,1,0:T(8,128)(2,1)}), bf16[16,128,256]{2,1,0:T(8,128)(2,1)S(1)}, u32[]{:S(2)}, u32[]{:S(2)}) %all-to-all-start.1) | async-done | bytes 1048608 | tf_op jit(solution)/shard_map/all_to_all | solution.py:61
  77.4 0.1 reduce_sum.70
  77.5 0.9 add_convert_fusion
  78.5 0.6 broadcast_in_dim.86
  79.1 5.2 %all-to-all-start.2 = ((f32[16,1,128]{2,1,0:T(1,128)}), f32[16,1,128]{2,1,0:T(1,128)S(1)}, u32[]{:S(2)}, u32[]{:S(2)}) async-start(f32[16,1,128]{2,1,0:T(1,128)} %broadcast_in_dim.86), calls=%async_computation.2 | async-start | bytes 16384 | tf_op jit(solution)/shard_map/all_to_all | solution.py:12
  84.4 0.8 dynamic_slice.7
  85.3 3.2 %all-to-all-done.2 = f32[16,1,128]{2,1,0:T(1,128)S(1)} async-done(((f32[16,1,128]{2,1,0:T(1,128)}), f32[16,1,128]{2,1,0:T(1,128)S(1)}, u32[]{:S(2)}, u32[]{:S(2)}) %all-to-all-start.2) | async-done | bytes 8224 | tf_op jit(solution)/shard_map/all_to_all | solution.py:12
  88.6 2.0 gather_fusion
  90.7 15.2 %all_to_all.26 = bf16[32,16,256]{2,1,0:T(8,128)(2,1)} all-to-all(bf16[32,16,256]{2,1,0:T(8,128)(2,1)S(1)} %broadcast_select_fusion), channel_id=1, replica_groups=mesh['sp'=32,'tp'=16] {'sp'}, dimensions={0} | all-to-all | bytes 524288 | tf_op jit(solution)/shard_map/all_to_all | solution.py:204
  106.0 45.2 %all-gather.2.cloned.1.call-done = bf16[32,16,4096]{2,1,0:T(8,128)(2,1)} async-done(((bf16[32,16,256]{2,1,0:T(8,128)(2,1)}), bf16[32,16,4096]{2,1,0:T(8,128)(2,1)}) %all-gather.2.cloned.1.call-update) | async-done | bytes 4194320 | tf_op jit(solution)/shard_map/all_gather | solution.py:205
  151.2 3.6 %fusion.5 = f32[32,16,128]{2,1,0:T(8,128)S(1)} fusion(bf16[32,16,4096]{2,1,0:T(8,128)(2,1)} %all-gather.2.cloned.1.call-done, bf16[1,4096,128]{2,1,0:T(8,128)(2,1)S(1)} %copy-done.2), kind=kOutput, calls=%fused_computation.12 | convolution fusion | flops 536870912 | bytes 5505024 | tf_op jit(solution)/shard_map/snd,df->snf/dot_general | solution.py:206
  154.8 2.5 fusion
  157.3 3.2 %convolution_convert_fusion = bf16[512,4096]{1,0:T(8,128)(2,1)} fusion(bf16[512,128]{1,0:T(8,128)(2,1)S(1)} %bitcast.140, bf16[1,128,4096]{2,1,0:T(8,128)(2,1)S(1)} %copy-done), kind=kOutput, calls=%fused_computation.2 | convolution fusion | flops 538968064 | bytes 5373952 | tf_op jit(solution)/shard_map/dot_general | solution.py:210
  160.8 65.8 %reduce-scatter.2.cloned.1.call-done = bf16[512,256]{1,0:T(8,128)(2,1)} async-done(((bf16[512,4096]{1,0:T(8,128)(2,1)}), bf16[512,256]{1,0:T(8,128)(2,1)}) %reduce-scatter.2.cloned.1.call-update) | async-done | bytes 262160 | tf_op jit(solution)/shard_map/reduce_scatter | solution.py:211
  226.6 9.7 %all-to-all-start.4 = ((bf16[32,16,256]{2,1,0:T(8,128)(2,1)}), bf16[32,16,256]{2,1,0:T(8,128)(2,1)S(1)}, u32[]{:S(2)}, u32[]{:S(2)}) async-start(bf16[32,16,256]{2,1,0:T(8,128)(2,1)} %bitcast.141), calls=%async_computation.5 | async-start | bytes 524288 | tf_op jit(solution)/shard_map/all_to_all | solution.py:215
  236.5 11.0 %all-to-all-done.4 = bf16[32,16,256]{2,1,0:T(8,128)(2,1)S(1)} async-done(((bf16[32,16,256]{2,1,0:T(8,128)(2,1)}), bf16[32,16,256]{2,1,0:T(8,128)(2,1)S(1)}, u32[]{:S(2)}, u32[]{:S(2)}) %all-to-all-start.4) | async-done | bytes 262176 | tf_op jit(solution)/shard_map/all_to_all | solution.py:215
  247.5 1.2 gather_fusion.1
  248.7 0.4 multiply_reduce_fusion
  249.1 0.6 fusion.11
  (65 shorter events, 2.6 us)
Async XLA Ops:
  6.5 150.8 %copy-start = (bf16[1,128,4096]{2,1,0:T(8,128)(2,1)S(1)}, bf16[1,128,4096]{2,1,0:T(8,128)(2,1)}, u32[]{:S(2)}) copy-start(bf16[1,128,4096]{2,1,0:T(8,128)(2,1)} %param.35) | copy-start | bytes 3145732
  13.0 15.5 %copy-start.9 = (f32[64]{0:T(128)S(1)}, f32[64]{0:T(128)}, u32[]{:S(2)}) copy-start(f32[64]{0:T(128)} %param.26) | copy-start | bytes 772
  13.4 26.3 %copy-start.5 = (f32[4,16,64]{2,1,0:T(8,128)S(1)}, f32[4,16,64]{2,1,0:T(8,128)}, u32[]{:S(2)}) copy-start(f32[4,16,64]{2,1,0:T(8,128)} %param.24) | copy-start | bytes 49156
  13.4 26.7 %copy-start.4 = (bf16[64,128]{1,0:T(8,128)(2,1)S(1)}, bf16[64,128]{1,0:T(8,128)(2,1)}, u32[]{:S(2)}) copy-start(bf16[64,128]{1,0:T(8,128)(2,1)} %param.18) | copy-start | bytes 49156
  13.4 26.7 %copy-start.6 = (f32[4,16,64]{2,1,0:T(8,128)S(1)}, f32[4,16,64]{2,1,0:T(8,128)}, u32[]{:S(2)}) copy-start(f32[4,16,64]{2,1,0:T(8,128)} %param.25) | copy-start | bytes 49156
  13.7 26.8 %copy-start.3 = (bf16[64,4096]{1,0:T(8,128)(2,1)S(1)}, bf16[64,4096]{1,0:T(8,128)(2,1)}, u32[]{:S(2)}) copy-start(bf16[64,4096]{1,0:T(8,128)(2,1)} %param.28) | copy-start | bytes 1572868
  15.6 22.2 %all-to-all-start = ((f32[32,1,1024]{2,1,0:T(1,128)}), f32[32,1,1024]{2,1,0:T(1,128)S(1)}, u32[]{:S(2)}, u32[]{:S(2)}) async-start(f32[32,1,1024]{2,1,0:T(1,128)} %reshape.198), calls=%async_computation | async-start | bytes 262144 | tf_op jit(solution)/shard_map/all_to_all | solution.py:12
  39.3 11.8 %copy-start.7 = (s32[128,2]{0,1:T(2,128)S(1)}, s32[128,2]{0,1:T(2,128)}, u32[]{:S(2)}) copy-start(s32[128,2]{0,1:T(2,128)} %param.31) | copy-start | bytes 3076
  42.0 109.2 %copy-start.2 = (bf16[1,4096,128]{2,1,0:T(8,128)(2,1)S(1)}, bf16[1,4096,128]{2,1,0:T(8,128)(2,1)}, u32[]{:S(2)}) copy-start(bf16[1,4096,128]{2,1,0:T(8,128)(2,1)} %param.33) | copy-start | bytes 3145732
  42.0 35.3 %all-to-all-start.1 = ((bf16[16,128,256]{2,1,0:T(8,128)(2,1)}), bf16[16,128,256]{2,1,0:T(8,128)(2,1)S(1)}, u32[]{:S(2)}, u32[]{:S(2)}) async-start(bf16[16,128,256]{2,1,0:T(8,128)(2,1)} %bitcast.68), calls=%async_computation.1 | async-start | bytes 2097152 | tf_op jit(solution)/shard_map/all_to_all | solution.py:61
  79.1 9.3 %all-to-all-start.2 = ((f32[16,1,128]{2,1,0:T(1,128)}), f32[16,1,128]{2,1,0:T(1,128)S(1)}, u32[]{:S(2)}, u32[]{:S(2)}) async-start(f32[16,1,128]{2,1,0:T(1,128)} %broadcast_in_dim.86), calls=%async_computation.2 | async-start | bytes 16384 | tf_op jit(solution)/shard_map/all_to_all | solution.py:12
  84.4 66.9 %all-gather.2.cloned.1.call-start = ((), (), s32[]{:S(2)}) async-start(), calls=%async_computation.6 | async-start | bytes 4456448 | tf_op jit(solution)/shard_map/all_gather | solution.py:205
  105.9 120.7 %reduce-scatter.2.cloned.1.call-start = ((), (), s32[]{:S(2)}) async-start(), calls=%async_computation.7 | async-start | bytes 4456448 | tf_op jit(solution)/shard_map/reduce_scatter | solution.py:211
  151.2 3.6 %copy-start.1 = (bf16[32,16,4096]{2,1,0:T(8,128)(2,1)S(1)}, bf16[32,16,4096]{2,1,0:T(8,128)(2,1)}, u32[]{:S(2)}) copy-start(bf16[32,16,4096]{2,1,0:T(8,128)(2,1)} %all-gather.2.cloned.1.call-done) | copy-start | bytes 12582916
  157.3 3.5 %copy-start.8 = (f32[128,2]{0,1:T(2,128)S(1)}, f32[128,2]{0,1:T(2,128)}, u32[]{:S(2)}) copy-start(f32[128,2]{0,1:T(2,128)} %param.32) | copy-start | bytes 3076
  226.6 20.9 %all-to-all-start.4 = ((bf16[32,16,256]{2,1,0:T(8,128)(2,1)}), bf16[32,16,256]{2,1,0:T(8,128)(2,1)S(1)}, u32[]{:S(2)}, u32[]{:S(2)}) async-start(bf16[32,16,256]{2,1,0:T(8,128)(2,1)} %bitcast.141), calls=%async_computation.5 | async-start | bytes 524288 | tf_op jit(solution)/shard_map/all_to_all | solution.py:215
Sparse Core Ops, SparseCore 0:
  106.1 45.1 all-gather.1
  160.6 65.9 reduce-scatter.1
where the time goes:
time: 257 us
  waiting for transfers between devices  159 us (62%)
  starting transfers between devices  37 us (14%)
  blocking collectives  15.2 us (6%)
  between operations  13.9 us (5%)
  matrix products  12.5 us (5%)
  local copies, waits for them, and re-layouts  9.55 us (4%)
  other arithmetic  9.4 us (4%)
    reduce_scatter x1, waiting for transfers between devices, per_device(): lax.psum_scatter(down_part.astype(f32).astype(jnp.bfloat16), 'tp', scatte...  65.8 us
    all_gather x1, waiting for transfers between devices, per_device(): piece = lax.all_gather(arrived, 'tp', axis=2, tiled=True)  45.2 us
    all_to_all x1, waiting for transfers between devices, sent_and_summed(): lax.all_to_all(in_blocks(array, dim, length), axis, 0, 0, tiled=True)  24.5 us
    all_to_all x2, starting transfers between devices, copy_for_each(): return lax.all_to_all(copies, axis, split_axis=0, concat_axis=0, tiled=True)  18.1 us
    all_to_all x1, blocking collectives, per_device(): lax.all_to_all(dispatch, 'sp', split_axis=0, concat_axis=0, tiled=True)  15.2 us
    all_to_all x2, waiting for transfers between devices, copy_for_each(): return lax.all_to_all(copies, axis, split_axis=0, concat_axis=0, tiled=True)  12.5 us
    all_to_all x1, waiting for transfers between devices, per_device(): lax.all_to_all(expert_out, 'sp', split_axis=0, concat_axis=0, tiled=True)  11 us
    all_to_all x1, starting transfers between devices, per_device(): lax.all_to_all(expert_out, 'sp', split_axis=0, concat_axis=0, tiled=True)  9.71 us
  transfers between devices with their start and end apart: 6, of which 6 were waited for; matrix products, arithmetic and copies ran while one was open for 1% of the time, Pallas kernels for 0%

commit v1 on v0

--- a/solution.py
+++ b/solution.py
@@ -1,3 +1,4 @@
+import functools
 import jax
 import jax.numpy as jnp
 from jax import lax
@@ -5,6 +6,13 @@
 
 EPS = 1e-06
 PRECISE_MODE = lax.Precision.HIGHEST
+
+
+def _solve_teams(field_in, across):
+    return jnp.concatenate(lax.all_gather(field_in, axis_name=across), 2)
+
+
+vector_keep_up = functools.partial(_solve_teams, across="tp")
 
 
 def copy_for_each(array, axis):
@@ -202,7 +210,7 @@
         experts, capacity, d_local
     )
     arrived = lax.all_to_all(dispatch, "sp", split_axis=0, concat_axis=0, tiled=True)
-    piece = lax.all_gather(arrived, "tp", axis=2, tiled=True)
+    piece = vector_keep_up(arrived)
     gate_part = jnp.einsum("snd,df->snf", piece, gate_w, preferred_element_type=f32)
     up_part = jnp.einsum("snd,df->snf", piece, up_w, preferred_element_type=f32)
     hidden = (jax.nn.silu(gate_part) * up_part).astype(bf16)

time: 257 us -> 249 us (0.969)
  waiting for transfers between devices: 159 us -> 151 us
  matrix products: 12.5 us -> 8.97 us
  local copies, waits for them, and re-layouts: 9.55 us -> 12.4 us
    all_gather x1, waiting for transfers between devices: 45.2 us -> 38.7 us  [_solve_teams(): return jnp.concatenate(lax.all_gather(field_in, axis_name=across), 2)]
    reshape x0 -> x1, local copies, waits for them, and re-layouts: none -> 2.82 us  [_solve_teams(): return jnp.concatenate(lax.all_gather(field_in, axis_name=across), 2)]
where the time goes in v1:
time: 249 us
  waiting for transfers between devices  151 us (61%)
  starting transfers between devices  37.5 us (15%)
  blocking collectives  15.2 us (6%)
  between operations  13.9 us (6%)
  local copies, waits for them, and re-layouts  12.4 us (5%)
  other arithmetic  9.4 us (4%)
  matrix products  8.97 us (4%)
    reduce_scatter x1, waiting for transfers between devices, per_device(): lax.psum_scatter(down_part.astype(f32).astype(jnp.bfloat16), 'tp', scatte...  64.6 us
    all_gather x1, waiting for transfers between devices, _solve_teams(): return jnp.concatenate(lax.all_gather(field_in, axis_name=across), 2)  38.7 us
    all_to_all x1, waiting for transfers between devices, sent_and_summed(): lax.all_to_all(in_blocks(array, dim, length), axis, 0, 0, tiled=True)  24.5 us
    all_to_all x2, starting transfers between devices, copy_for_each(): return lax.all_to_all(copies, axis, split_axis=0, concat_axis=0, tiled=True)  18.1 us
    all_to_all x1, blocking collectives, per_device(): lax.all_to_all(dispatch, 'sp', split_axis=0, concat_axis=0, tiled=True)  15.2 us
    all_to_all x2, waiting for transfers between devices, copy_for_each(): return lax.all_to_all(copies, axis, split_axis=0, concat_axis=0, tiled=True)  12.5 us
    all_to_all x1, waiting for transfers between devices, per_device(): lax.all_to_all(expert_out, 'sp', split_axis=0, concat_axis=0, tiled=True)  11 us
    all_to_all x1, starting transfers between devices, per_device(): lax.all_to_all(expert_out, 'sp', split_axis=0, concat_axis=0, tiled=True)  10.1 us
  transfers between devices with their start and end apart: 6, of which 6 were waited for; matrix products, arithmetic and copies ran while one was open for 1% of the time, Pallas kernels for 0%

profile of v1, /device:TPU:25, one launch (start us, length us, event | category | flops | bytes accessed | tf_op | source)
XLA Modules:
  0.0 248.6 jit_solution(3410195243867221849)
XLA Ops:
  6.5 0.7 exp.13
  7.3 0.8 fusion.57
  8.1 1.1 fusion.42
  9.2 1.1 fusion.46
  10.3 0.9 subtract_add_fusion.6
  11.2 1.0 add_add_fusion.5
  12.3 0.2 add_add_fusion.4
  12.7 0.2 add_add_fusion.3
  13.1 0.2 add_add_fusion.2
  13.4 0.2 add_add_fusion.1
  13.8 0.2 add_add_fusion
  14.0 0.2 multiply_subtract_fusion
  14.2 0.3 slice_reduce_fusion.1
  14.5 0.3 slice_reduce_fusion
  14.8 0.8 reshape.207
  15.6 12.9 %all-to-all-start = ((f32[32,1,1024]{2,1,0:T(1,128)}), f32[32,1,1024]{2,1,0:T(1,128)S(1)}, u32[]{:S(2)}, u32[]{:S(2)}) async-start(f32[32,1,1024]{2,1,0:T(1,128)} %reshape.207), calls=%async_computation | async-start | bytes 262144 | tf_op jit(solution)/shard_map/all_to_all | solution.py:20
  28.6 9.2 %all-to-all-done = f32[32,1,1024]{2,1,0:T(1,128)S(1)} async-done(((f32[32,1,1024]{2,1,0:T(1,128)}), f32[32,1,1024]{2,1,0:T(1,128)S(1)}, u32[]{:S(2)}, u32[]{:S(2)}) %all-to-all-start) | async-done | bytes 131104 | tf_op jit(solution)/shard_map/all_to_all | solution.py:20
  37.9 0.5 broadcast.191
  38.4 1.0 reduce.12
  39.8 0.3 fusion.16
  40.1 0.4 fusion.36
  40.5 0.5 convolution_convert_fusion.1
  41.0 1.1 copy.125
  42.1 9.0 %all-to-all-start.1 = ((bf16[16,128,256]{2,1,0:T(8,128)(2,1)}), bf16[16,128,256]{2,1,0:T(8,128)(2,1)S(1)}, u32[]{:S(2)}, u32[]{:S(2)}) async-start(bf16[16,128,256]{2,1,0:T(8,128)(2,1)} %bitcast.73), calls=%async_computation.1 | async-start | bytes 2097152 | tf_op jit(solution)/shard_map/all_to_all | solution.py:69
  51.5 0.6 reduce-window.6
  52.1 0.2 slice_reduce_fusion.4
  52.4 0.2 fusion.7
  52.6 0.2 select_reduce_fusion
  52.8 24.5 %all-to-all-done.1 = bf16[16,128,256]{2,1,0:T(8,128)(2,1)S(1)} async-done(((bf16[16,128,256]{2,1,0:T(8,128)(2,1)}), bf16[16,128,256]{2,1,0:T(8,128)(2,1)S(1)}, u32[]{:S(2)}, u32[]{:S(2)}) %all-to-all-start.1) | async-done | bytes 1048608 | tf_op jit(solution)/shard_map/all_to_all | solution.py:69
  77.4 0.9 add_convert_fusion
  78.4 0.6 broadcast_in_dim.86
  79.0 5.2 %all-to-all-start.2 = ((f32[16,1,128]{2,1,0:T(1,128)}), f32[16,1,128]{2,1,0:T(1,128)S(1)}, u32[]{:S(2)}, u32[]{:S(2)}) async-start(f32[16,1,128]{2,1,0:T(1,128)} %broadcast_in_dim.86), calls=%async_computation.2 | async-start | bytes 16384 | tf_op jit(solution)/shard_map/all_to_all | solution.py:20
  84.3 0.8 dynamic_slice.7
  85.1 3.2 %all-to-all-done.2 = f32[16,1,128]{2,1,0:T(1,128)S(1)} async-done(((f32[16,1,128]{2,1,0:T(1,128)}), f32[16,1,128]{2,1,0:T(1,128)S(1)}, u32[]{:S(2)}, u32[]{:S(2)}) %all-to-all-start.2) | async-done | bytes 8224 | tf_op jit(solution)/shard_map/all_to_all | solution.py:20
  88.5 2.0 gather_fusion
  90.6 15.2 %all_to_all.26 = bf16[32,16,256]{2,1,0:T(8,128)(2,1)} all-to-all(bf16[32,16,256]{2,1,0:T(8,128)(2,1)S(1)} %broadcast_select_fusion), channel_id=1, replica_groups=mesh['sp'=32,'tp'=16] {'sp'}, dimensions={0} | all-to-all | bytes 524288 | tf_op jit(solution)/shard_map/all_to_all | solution.py:212
  105.8 0.2 reduce-scatter.2.cloned.1.call-start
  106.0 38.7 %all-gather.3.cloned.1.call-done = bf16[512,16,256]{2,1,0:T(8,128)(2,1)} async-done(((bf16[32,16,256]{2,1,0:T(8,128)(2,1)}), bf16[512,16,256]{2,1,0:T(8,128)(2,1)}) %all-gather.3.cloned.1.call-update) | async-done | bytes 4194320 | tf_op jit(solution)/shard_map/all_gather | solution.py:12
  144.8 2.8 %copy.122 = bf16[16,32,2,8,256]{4,3,0,2,1:T(8,128)(2,1)S(1)} copy(bf16[16,32,2,8,256]{4,3,2,1,0:T(8,128)(2,1)} %bitcast.105) | data formatting | bytes 8388608 | tf_op jit(solution)/shard_map/reshape | solution.py:12
  147.6 1.2 fusion.5
  148.9 1.3 fusion
  150.2 3.2 %convolution_convert_fusion = bf16[512,4096]{1,0:T(8,128)(2,1)} fusion(bf16[512,128]{1,0:T(8,128)(2,1)S(1)} %bitcast.148, bf16[1,128,4096]{2,1,0:T(8,128)(2,1)S(1)} %copy-done), kind=kOutput, calls=%fused_computation.2 | convolution fusion | flops 538968064 | bytes 5373952 | tf_op jit(solution)/shard_map/dot_general | solution.py:218
  153.7 64.6 %reduce-scatter.2.cloned.1.call-done = bf16[512,256]{1,0:T(8,128)(2,1)} async-done(((bf16[512,4096]{1,0:T(8,128)(2,1)}), bf16[512,256]{1,0:T(8,128)(2,1)}) %reduce-scatter.2.cloned.1.call-update) | async-done | bytes 262160 | tf_op jit(solution)/shard_map/reduce_scatter | solution.py:219
  218.3 10.1 %all-to-all-start.4 = ((bf16[32,16,256]{2,1,0:T(8,128)(2,1)}), bf16[32,16,256]{2,1,0:T(8,128)(2,1)S(1)}, u32[]{:S(2)}, u32[]{:S(2)}) async-start(bf16[32,16,256]{2,1,0:T(8,128)(2,1)} %bitcast.149), calls=%async_computation.5 | async-start | bytes 524288 | tf_op jit(solution)/shard_map/all_to_all | solution.py:223
  228.5 11.0 %all-to-all-done.4 = bf16[32,16,256]{2,1,0:T(8,128)(2,1)S(1)} async-done(((bf16[32,16,256]{2,1,0:T(8,128)(2,1)}), bf16[32,16,256]{2,1,0:T(8,128)(2,1)S(1)}, u32[]{:S(2)}, u32[]{:S(2)}) %all-to-all-start.4) | async-done | bytes 262176 | tf_op jit(solution)/shard_map/all_to_all | solution.py:223
  239.5 1.2 gather_fusion.1
  240.7 0.4 multiply_reduce_fusion
  241.2 0.6 fusion.11
  (66 shorter events, 2.9 us)
Async XLA Ops:
  6.5 143.6 %copy-start = (bf16[1,128,4096]{2,1,0:T(8,128)(2,1)S(1)}, bf16[1,128,4096]{2,1,0:T(8,128)(2,1)}, u32[]{:S(2)}) copy-start(bf16[1,128,4096]{2,1,0:T(8,128)(2,1)} %param.35) | copy-start | bytes 3145732
  13.0 15.5 %copy-start.8 = (f32[64]{0:T(128)S(1)}, f32[64]{0:T(128)}, u32[]{:S(2)}) copy-start(f32[64]{0:T(128)} %param.26) | copy-start | bytes 772
  13.4 26.3 %copy-start.4 = (f32[4,16,64]{2,1,0:T(8,128)S(1)}, f32[4,16,64]{2,1,0:T(8,128)}, u32[]{:S(2)}) copy-start(f32[4,16,64]{2,1,0:T(8,128)} %param.24) | copy-start | bytes 49156
  13.4 26.7 %copy-start.3 = (bf16[64,128]{1,0:T(8,128)(2,1)S(1)}, bf16[64,128]{1,0:T(8,128)(2,1)}, u32[]{:S(2)}) copy-start(bf16[64,128]{1,0:T(8,128)(2,1)} %param.18) | copy-start | bytes 49156
  13.4 26.7 %copy-start.5 = (f32[4,16,64]{2,1,0:T(8,128)S(1)}, f32[4,16,64]{2,1,0:T(8,128)}, u32[]{:S(2)}) copy-start(f32[4,16,64]{2,1,0:T(8,128)} %param.25) | copy-start | bytes 49156
  13.7 26.8 %copy-start.2 = (bf16[64,4096]{1,0:T(8,128)(2,1)S(1)}, bf16[64,4096]{1,0:T(8,128)(2,1)}, u32[]{:S(2)}) copy-start(bf16[64,4096]{1,0:T(8,128)(2,1)} %param.28) | copy-start | bytes 1572868
  15.6 22.2 %all-to-all-start = ((f32[32,1,1024]{2,1,0:T(1,128)}), f32[32,1,1024]{2,1,0:T(1,128)S(1)}, u32[]{:S(2)}, u32[]{:S(2)}) async-start(f32[32,1,1024]{2,1,0:T(1,128)} %reshape.207), calls=%async_computation | async-start | bytes 262144 | tf_op jit(solution)/shard_map/all_to_all | solution.py:20
  39.4 11.7 %copy-start.6 = (s32[128,2]{0,1:T(2,128)S(1)}, s32[128,2]{0,1:T(2,128)}, u32[]{:S(2)}) copy-start(s32[128,2]{0,1:T(2,128)} %param.31) | copy-start | bytes 3076
  42.1 35.2 %all-to-all-start.1 = ((bf16[16,128,256]{2,1,0:T(8,128)(2,1)}), bf16[16,128,256]{2,1,0:T(8,128)(2,1)S(1)}, u32[]{:S(2)}, u32[]{:S(2)}) async-start(bf16[16,128,256]{2,1,0:T(8,128)(2,1)} %bitcast.73), calls=%async_computation.1 | async-start | bytes 2097152 | tf_op jit(solution)/shard_map/all_to_all | solution.py:69
  79.0 9.3 %all-to-all-start.2 = ((f32[16,1,128]{2,1,0:T(1,128)}), f32[16,1,128]{2,1,0:T(1,128)S(1)}, u32[]{:S(2)}, u32[]{:S(2)}) async-start(f32[16,1,128]{2,1,0:T(1,128)} %broadcast_in_dim.86), calls=%async_computation.2 | async-start | bytes 16384 | tf_op jit(solution)/shard_map/all_to_all | solution.py:20
  84.2 60.5 %all-gather.3.cloned.1.call-start = ((), (), s32[]{:S(2)}) async-start(), calls=%async_computation.7 | async-start | bytes 4456448 | tf_op jit(solution)/shard_map/all_gather | solution.py:12
  105.8 112.5 %reduce-scatter.2.cloned.1.call-start = ((), (), s32[]{:S(2)}) async-start(), calls=%async_computation.6 | async-start | bytes 4456448 | tf_op jit(solution)/shard_map/reduce_scatter | solution.py:219
  144.8 2.8 %copy-start.1 = (bf16[1,4096,128]{2,1,0:T(8,128)(2,1)S(1)}, bf16[1,4096,128]{2,1,0:T(8,128)(2,1)}, u32[]{:S(2)}) copy-start(bf16[1,4096,128]{2,1,0:T(8,128)(2,1)} %param.33) | copy-start | bytes 3145732
  147.6 1.3 copy-start.9
  150.2 3.5 %copy-start.7 = (f32[128,2]{0,1:T(2,128)S(1)}, f32[128,2]{0,1:T(2,128)}, u32[]{:S(2)}) copy-start(f32[128,2]{0,1:T(2,128)} %param.32) | copy-start | bytes 3076
  218.3 21.2 %all-to-all-start.4 = ((bf16[32,16,256]{2,1,0:T(8,128)(2,1)}), bf16[32,16,256]{2,1,0:T(8,128)(2,1)S(1)}, u32[]{:S(2)}, u32[]{:S(2)}) async-start(bf16[32,16,256]{2,1,0:T(8,128)(2,1)} %bitcast.149), calls=%async_computation.5 | async-start | bytes 524288 | tf_op jit(solution)/shard_map/all_to_all | solution.py:223
Sparse Core Ops, SparseCore 0:
  105.9 38.7 all-gather.2
  153.5 64.7 reduce-scatter.1
